TPU v7x, 32 devices: a whole 2x2x4 slice. The times are simulated.
32 devices in a mesh: grp: 2 (over y), ep: 4 (over z), tp: 4 (over x, core).
Axes of the slice: x: 2, y: 2, z: 4, core: 2. Of those that a mesh axis runs over, the one named last changes fastest.
Arguments:
- query: bfloat16 [8192, 1024], P(('grp', 'ep'), 'tp'), parts along dimension 0, may hold values from -6 to 6
- forget_gate_logits: bfloat16 [8192, 1024], P(('grp', 'ep'), 'tp'), parts along dimension 0, may hold values from -8 to 8
- value: bfloat16 [8192, 1024], P(('grp', 'ep'), 'tp'), parts along dimension 0, may hold values from -6 to 6
- forget_lower_margin: float32 [2, 1024], P(None, 'tp'), may hold values from -30 to -2
- position_log_decay: float32 [8, 8192], P('tp', ('grp', 'ep')), parts along dimension 1, may hold values from -1.5 to 0
- head_norm_gain: float32 [128], replicated, may hold values from 0.1 to 1.9
- mixer_output_weight: bfloat16 [1024, 2048], P('tp'), may hold values from -0.1875 to 0.1875
- second_batch_tokens: bfloat16 [4096, 2048], P(('grp', 'ep', 'tp')), parts along dimension 0, may hold values from -60 to 60
- expert_norm_gain: float32 [2048], replicated, may hold values from 0.1 to 1.9
- routes: int32 [4096, 2], P(('grp', 'ep', 'tp')), parts along dimension 0, may hold values from 0 to 3, all different within a row; in each aligned block of 128 rows (0 to 127, 128 to 255, ...) at most 96 rows name the same one
- chosen_expert_weight: float32 [4096, 2], P(('grp', 'ep', 'tp')), parts along dimension 0, may hold values from 0.2 to 1
- gate_weight: bfloat16 [4, 2048, 2048], P('ep', None, 'tp'), may hold values from -0.3125 to 0.3125
- up_weight: bfloat16 [4, 2048, 2048], P('ep', None, 'tp'), may hold values from -0.3125 to 0.3125
- down_weight: bfloat16 [4, 2048, 2048], P('ep', 'tp'), may hold values from -0.02734375 to 0.02734375
Outputs:
- first_mixer_output: bfloat16 [8192, 2048], P(('grp', 'ep', 'tp')), parts along dimension 0
- moe_out: bfloat16 [4096, 2048], P(('grp', 'ep', 'tp')), parts along dimension 0
There are 2 independent parts, one for each index of `grp`. A program takes and returns all parts, laid end to end along the dimension named above; an argument that names none is the same for every part. Nothing has to cross between parts.
Inputs may be any that keep to these rules, and one draw needn't show every extreme that they name: `routes`: each row names 2 different experts. Among the rows of one device no expert is named by more than 96 rows, and in every draw some expert is named by exactly 96 rows of some device.
All inputs are finite; a program needn't handle non-finite values.
Results may differ from a plain program's by a relative error of at most 0.015.
Values may be sent and summed in bfloat16 or wider, within the bound.
A program may use at most 128 MiB of HBM per device.

v0:
```python
import jax
import jax.numpy as jnp
from jax import lax
from jax.sharding import PartitionSpec as P

HEAD_CHANNELS = 128
BLK = 128
NORM_EPS = 1e-06
CLAMP_LIMIT = 7.0
SIGMOID_SCALE = 1.702
PRECISE = lax.Precision.HIGHEST


def carried_in(value, axis, combine, identity, reverse):
    length, position = (lax.axis_size(axis), lax.axis_index(axis))
    everything = jax.tree.map(
        lambda part, kind: lax.all_gather(part.astype(kind), axis),
        value,
        (jnp.bfloat16, jnp.bfloat16),
    )
    start = jax.tree.map(
        lambda part, zero: jnp.broadcast_to(jnp.asarray(zero, part.dtype), part.shape),
        value,
        identity,
    )

    def turn(k, before):
        at = length - 1 - k if reverse else k
        reached = at > position if reverse else at < position
        new = combine(
            before, jax.tree.map(lambda part, own: part[at].astype(own.dtype), everything, value)
        )
        return jax.tree.map(lambda a, b: jnp.where(reached, a, b), new, before)

    return lax.fori_loop(0, length, turn, start)


def clamped_unit(gate_pre, up_pre):
    gate_pre = jnp.minimum(gate_pre, CLAMP_LIMIT)
    up_pre = jnp.clip(up_pre, -CLAMP_LIMIT, CLAMP_LIMIT)
    return (up_pre + 1.0) * gate_pre * jax.nn.sigmoid(SIGMOID_SCALE * gate_pre)


def local_recurrence(queries, ending_state, values, forget_log_rates):
    sequence_length, number_of_heads, channels = queries.shape
    nblocks = sequence_length // BLK

    def to_blocks(array):
        return array.reshape(nblocks, BLK, number_of_heads, array.shape[-1])

    query_blocks = to_blocks(queries)
    key_blocks = to_blocks(ending_state)
    value_blocks = to_blocks(values)
    cumul = jnp.cumsum(to_blocks(forget_log_rates), axis=1)
    block_last = cumul[:, -1]
    query_in = query_blocks * jnp.exp(cumul)
    key_in = key_blocks * jnp.exp(-cumul)
    key_state = key_blocks * jnp.exp(block_last[:, None] - cumul)
    lower = jnp.tril(jnp.ones((BLK, BLK), jnp.float32))
    scores = jnp.einsum("nchd,nshd->nhcs", query_in, key_in, precision=PRECISE) * lower
    inner = jnp.einsum("nhcs,nshv->nchv", scores, value_blocks, precision=PRECISE)
    increments = jnp.einsum("nshd,nshv->nhdv", key_state, value_blocks, precision=PRECISE)

    def advance(state, inputs):
        decay, increment = inputs
        return (state * decay[..., None] + increment, state)

    initial = jnp.zeros((number_of_heads, channels, values.shape[-1]), jnp.float32)
    final_state, before = lax.scan(advance, initial, (jnp.exp(block_last), increments))
    outer = jnp.einsum("nchd,nhdv->nchv", query_in, before, precision=PRECISE)
    output = (inner + outer).reshape(sequence_length, number_of_heads, values.shape[-1])
    offsets = jnp.cumsum(block_last, axis=0) - block_last
    carried_query = (query_blocks * jnp.exp(cumul + offsets[:, None])).reshape(
        sequence_length, number_of_heads, channels
    )
    total_log = jnp.sum(block_last, axis=0)
    return (output, final_state, total_log, carried_query)


def chain_combine(earlier, later):
    return (earlier[0] * later[0], earlier[1] * later[0][..., None] + later[1])


def mixer_head_states(
    query, forget_gate_logits, value, forget_lower_margin, position_log_decay, head_norm_gain
):
    sequence_length = query.shape[0]
    number_of_heads = query.shape[1] // HEAD_CHANNELS
    queries = jax.nn.silu(query.astype(jnp.float32)).reshape(
        sequence_length, number_of_heads, HEAD_CHANNELS
    ) * HEAD_CHANNELS ** (-0.5)
    values = value.astype(jnp.float32).reshape(sequence_length, number_of_heads, HEAD_CHANNELS)
    shutting = jax.nn.sigmoid(-forget_gate_logits.astype(jnp.float32))
    decay_spikes = jnp.transpose(position_log_decay)[:, :, None]
    ending_state = jnp.exp(forget_lower_margin[0])[None, :] * shutting
    forget_log_rates = (
        jnp.log1p(-ending_state).reshape(sequence_length, number_of_heads, HEAD_CHANNELS)
        + decay_spikes
    )
    ending_state = ending_state.reshape(sequence_length, number_of_heads, HEAD_CHANNELS)
    output, final_state, total_log, carried = local_recurrence(
        queries, ending_state, values, forget_log_rates
    )
    identity = (jnp.ones_like(total_log), jnp.zeros_like(final_state))
    entering = carried_in((jnp.exp(total_log), final_state), "ep", chain_combine, identity, False)[
        1
    ]
    forward = output + jnp.einsum("lhd,hdv->lhv", carried, entering, precision=PRECISE)
    ending_state = jnp.exp(forget_lower_margin[1])[None, :] * shutting
    forget_log_rates = (
        jnp.log1p(-ending_state).reshape(sequence_length, number_of_heads, HEAD_CHANNELS)
        + decay_spikes
    )
    ending_state = ending_state.reshape(sequence_length, number_of_heads, HEAD_CHANNELS)
    output, final_state, total_log, carried = local_recurrence(
        jnp.flip(queries, 0),
        jnp.flip(ending_state, 0),
        jnp.flip(values, 0),
        jnp.flip(forget_log_rates, 0),
    )
    entering = carried_in((jnp.exp(total_log), final_state), "ep", chain_combine, identity, True)[1]
    backward = jnp.flip(
        output + jnp.einsum("lhd,hdv->lhv", carried, entering, precision=PRECISE), 0
    )
    mix = forward + backward
    scaled = (
        mix * lax.rsqrt(jnp.mean(mix * mix, axis=-1, keepdims=True) + NORM_EPS) * head_norm_gain
    )
    return scaled.reshape(sequence_length, number_of_heads * HEAD_CHANNELS).astype(jnp.bfloat16)


def body(
    query,
    forget_gate_logits,
    value,
    forget_lower_margin,
    position_log_decay,
    head_norm_gain,
    mixer_output_weight,
    second_batch_tokens,
    expert_norm_gain,
    routes,
    chosen_expert_weight,
    gate_weight,
    up_weight,
    down_weight,
):
    head_outputs = mixer_head_states(
        query, forget_gate_logits, value, forget_lower_margin, position_log_decay, head_norm_gain
    )
    tokens, top_count = routes.shape
    features = second_batch_tokens.shape[1]
    n_ep = lax.axis_size("ep")
    n_tp = lax.axis_size("tp")
    capacity = (3 * tokens * top_count + 2 * n_ep - 1) // (2 * n_ep)
    tokens_f = second_batch_tokens.astype(jnp.float32)
    normed = (
        tokens_f
        * lax.rsqrt(jnp.mean(tokens_f * tokens_f, axis=-1, keepdims=True) + NORM_EPS)
        * expert_norm_gain
    ).astype(jnp.bfloat16)
    flat_routes = routes.reshape(-1)
    onehot = (flat_routes[:, None] == jnp.arange(n_ep, dtype=jnp.int32)[None, :]).astype(jnp.int32)
    ranking = jnp.cumsum(onehot, axis=0) - onehot
    slot_index = jnp.sum(ranking * onehot, axis=1)
    destination = flat_routes * capacity + slot_index
    source = (
        jnp.full((n_ep * capacity,), tokens, jnp.int32)
        .at[destination]
        .set(jnp.arange(tokens * top_count, dtype=jnp.int32) // top_count)
    )
    padded = jnp.concatenate([normed, jnp.zeros((1, features), jnp.bfloat16)], axis=0)
    send = padded[source]
    expert_block = n_ep * capacity
    copies = jnp.broadcast_to(
        send.reshape(n_ep, 1, capacity, features), (n_ep, n_tp, capacity, features)
    ).reshape(n_ep * n_tp * capacity, features)
    arrived = lax.all_to_all(copies, ("ep", "tp"), split_axis=0, concat_axis=0, tiled=True)
    gate_pre = jnp.dot(arrived, gate_weight[0], preferred_element_type=jnp.float32)
    up_pre = jnp.dot(arrived, up_weight[0], preferred_element_type=jnp.float32)
    hidden = clamped_unit(gate_pre, up_pre).astype(jnp.bfloat16)
    picked = head_outputs
    first_mixer_output = lax.psum_scatter(
        jnp.dot(picked, mixer_output_weight, preferred_element_type=jnp.float32).astype(
            jnp.bfloat16
        ),
        "tp",
        scatter_dimension=0,
        tiled=True,
    )
    block_count = expert_block * lax.axis_size("tp") // expert_block
    grid_view = hidden.reshape(n_ep, n_tp, capacity, hidden.shape[-1])
    picked = grid_view
    picked = jnp.moveaxis(picked, 1, 0).reshape(block_count * expert_block, hidden.shape[-1])
    expert_sum = lax.psum_scatter(
        jnp.dot(picked, down_weight[0], preferred_element_type=jnp.float32).astype(jnp.bfloat16),
        "tp",
        scatter_dimension=0,
        tiled=True,
    )
    returned = lax.all_to_all(expert_sum, "ep", split_axis=0, concat_axis=0, tiled=True)
    gathered = returned[destination].reshape(tokens, top_count, features)
    moe_out = jnp.sum(
        chosen_expert_weight[:, :, None] * gathered.astype(jnp.float32), axis=1
    ).astype(jnp.bfloat16)
    return (first_mixer_output, moe_out)


def solution(mesh):
    return jax.shard_map(
        body,
        mesh=mesh,
        in_specs=(
            P(("grp", "ep"), "tp"),
            P(("grp", "ep"), "tp"),
            P(("grp", "ep"), "tp"),
            P(None, "tp"),
            P("tp", ("grp", "ep")),
            P(),
            P("tp", None),
            P(("grp", "ep", "tp"), None),
            P(),
            P(("grp", "ep", "tp"), None),
            P(("grp", "ep", "tp"), None),
            P("ep", None, "tp"),
            P("ep", None, "tp"),
            P("ep", "tp", None),
        ),
        out_specs=(P(("grp", "ep", "tp"), None), P(("grp", "ep", "tp"), None)),
        check_vma=False,
    )
```

profile of v0, /device:TPU:0, one launch (start us, length us, event | category | flops | bytes accessed | tf_op | source)
XLA Modules:
  0.0 379.8 jit_solution(997884726654975377)
XLA Ops:
  15.0 3.1 gather_fusion
  18.0 4.9 %broadcast_in_dim.32 = bf16[4,4,96,2048]{3,2,1,0:T(8,128)(2,1)} broadcast(bf16[4,96,2048]{2,1,0:T(8,128)(2,1)} %bitcast.183), dimensions={0,2,3} | broadcast | bytes 7864320 | tf_op jit(solution)/shard_map/broadcast_in_dim | solution.py:175
  22.9 7.6 %all-to-all-start = ((bf16[16,96,2048]{2,1,0:T(8,128)(2,1)}), bf16[16,96,2048]{2,1,0:T(8,128)(2,1)}, u32[]{:S(2)}, u32[]{:S(2)}) async-start(bf16[16,96,2048]{2,1,0:T(8,128)(2,1)} %bitcast.178), calls=%async_computation.1 | async-start | bytes 12582912 | tf_op jit(solution)/shard_map/all_to_all | solution.py:178
  31.1 2.3 log-plus-one_bitcast_fusion
  35.2 1.6 fusion.31
  36.8 2.8 copy.175
  39.6 2.5 copy.123
  42.1 2.0 copy.118
  44.2 2.4 multiply_bitcast_fusion
  47.8 2.6 copy.122
  50.4 2.0 reshape_reshape.7
  52.4 3.4 exponential_multiply_fusion.2
  55.9 2.4 convolution_multiply_fusion.1
  58.3 1.6 convolution_bitcast_fusion.5
  59.9 2.0 fusion.25
  63.0 14.2 %while.56 = (s32[]{:T(128)}, f32[2,128,128]{2,1,0:T(8,128)S(1)}, f32[8,2,128,128]{3,2,1,0:T(8,128)}, f32[8,2,128]{2,0,1:T(8,128)S(1)}, f32[8,2,128,128]{3,2,1,0:T(8,128)}, /*index=5*/s32[]{:T(128)}, s32[]{:T(128)}) while((s32[]{:T(128)}, f32[2,128,128]{2,1,0:T(8,128)S(1)}, f32[8,2,128,128]{3,2,1,0:T(8,128)}, ...), condition=%wide.region_2.3_spmd.clone, body=%wide.region_1.2_spmd.clone.sunk | while | flops 131075 | bytes 659040 | solution.py:69
  77.2 67.3 %all-to-all-done = bf16[16,96,2048]{2,1,0:T(8,128)(2,1)} async-done(((bf16[16,96,2048]{2,1,0:T(8,128)(2,1)}), bf16[16,96,2048]{2,1,0:T(8,128)(2,1)}, u32[]{:S(2)}, u32[]{:S(2)}) %all-to-all-start) | async-done | bytes 6291488 | tf_op jit(solution)/shard_map/all_to_all | solution.py:178
  144.6 6.3 %convolution_minimum_fusion = f32[1536,512]{1,0:T(8,128)S(1)} fusion(bf16[1536,2048]{1,0:T(8,128)(2,1)} %bitcast.35, bf16[1,2048,512]{2,1,0:T(8,128)(2,1)} %param.33), kind=kOutput, calls=%fused_computation.18 | convolution fusion | flops 3222011904 | bytes 11534336 | tf_op jit(solution)/shard_map/dot_general | solution.py:179
  150.9 6.9 %fusion.5 = bf16[1536,512]{1,0:T(8,128)(2,1)S(1)} fusion(f32[1536,512]{1,0:T(8,128)S(1)} %convolution_minimum_fusion, bf16[1536,2048]{1,0:T(8,128)(2,1)} %bitcast.35, bf16[1,2048,512]{2,1,0:T(8,128)(2,1)S(1)} %copy-done.22), kind=kOutput, calls=%fused_computation.22 | convolution fusion | flops 3228303360 | bytes 13107200 | tf_op jit(solution)/shard_map/dot_general | solution.py:180
  157.9 5.4 %convolution_convert_fusion = bf16[1536,2048]{1,0:T(8,128)(2,1)} fusion(bf16[1536,512]{1,0:T(8,128)(2,1)S(1)} %bitcast.199, bf16[1,512,2048]{2,1,0:T(8,128)(2,1)S(1)} %copy-done), kind=kOutput, calls=%fused_computation.15 | convolution fusion | flops 3224371200 | bytes 9961472 | tf_op jit(solution)/shard_map/dot_general | solution.py:196
  164.9 2.1 fusion.13
  171.2 1.7 rev.17
  174.1 1.9 fusion.23
  177.0 7.5 %rev.18 = f32[1024,2,128]{0,2,1:T(8,128)S(1)} reverse(f32[1024,2,128]{0,2,1:T(8,128)} %bitcast.193), dimensions={0} | reverse | bytes 2097152 | tf_op jit(solution)/shard_map/jit(_flip)/rev | solution.py:117
  188.8 5.9 %rev.19 = f32[1024,2,128]{0,2,1:T(8,128)} reverse(bf16[1024,2,128]{0,2,1:T(8,128)(2,1)S(1)} %bitcast.196), dimensions={0} | reverse | bytes 1572864 | tf_op jit(solution)/shard_map/jit(_flip)/rev | solution.py:118
  194.8 1.9 copy.147
  198.2 4.5 %exponential_multiply_fusion = (f32[8,128,2,128]{3,0,1,2:T(8,128)S(1)}, f32[8,128,2,128]{3,0,1,2:T(8,128)S(1)}, f32[8,128,2,128]{3,0,1,2:T(8,128)}, f32[8,128,2,128]{3,0,1,2:T(8,128)S(1)}) fusion(f32[8,128,2,128]{3,0,1,2:T(8,128)} %copy-done.8, f32[8,128,2,128]{3,1,0,2:T(8,128)} %bitcast.184, f32[8,2,128]{2,0,1:T(8,128)S(1)} %get-tuple-element.453, ...), kind=kLoop, calls=%fused_computation.63 | loop fusion | flops 1572864 | bytes 7356416 | tf_op jit(solution)/shard_map/mul | solution.py:58
  202.7 2.4 convolution_multiply_fusion
  205.1 2.2 convolution_bitcast_fusion.2
  207.3 2.9 fusion.20
  211.3 13.7 %while.58 = (s32[]{:T(128)}, f32[2,128,128]{2,1,0:T(8,128)S(1)}, f32[8,2,128,128]{3,2,1,0:T(8,128)}, f32[8,2,128]{2,0,1:T(8,128)S(1)}, f32[8,2,128,128]{3,2,1,0:T(8,128)}, /*index=5*/s32[]{:T(128)}, s32[]{:T(128)}) while((s32[]{:T(128)}, f32[2,128,128]{2,1,0:T(8,128)S(1)}, f32[8,2,128,128]{3,2,1,0:T(8,128)}, ...), condition=%wide.region_9.10_spmd.clone, body=%wide.region_8.9_spmd.clone.sunk | while | flops 131075 | bytes 659040 | solution.py:69
  225.0 3.4 fusion.10
  228.4 1.8 copy.154
  232.6 2.5 copy.156
  235.2 31.3 %all-gather.5 = bf16[4,2,128]{2,1,0:T(2,128)(2,1)S(1)} all-gather(bf16[1,2,128]{2,1,0:T(2,128)(2,1)S(1)} %fusion.50), channel_id=4, replica_groups=mesh['grp'=2,'ep'=4,'tp'=4] {'ep'}, dimensions={0}, use_global_device_ids=true | all-gather | bytes 2560 | tf_op jit(solution)/shard_map/all_gather | solution.py:17
  266.4 13.9 %all-gather.3 = bf16[8,128,128]{2,1,0:T(8,128)(2,1)S(1)} all-gather(bf16[2,128,128]{2,1,0:T(8,128)(2,1)S(1)} %convert_element_type.137), channel_id=5, replica_groups=mesh['grp'=2,'ep'=4,'tp'=4] {'ep'}, dimensions={0}, use_global_device_ids=true | all-gather | bytes 327680 | tf_op jit(solution)/shard_map/all_gather | solution.py:17
  281.2 3.6 fusion.9
  284.9 9.4 %rev.20 = f32[1024,2,128]{0,2,1:T(8,128)} reverse(f32[1024,2,128]{0,2,1:T(8,128)} %fusion.9), dimensions={0} | reverse | bytes 2097152 | tf_op jit(solution)/shard_map/jit(_flip)/rev | solution.py:122
  295.5 2.7 copy.134
  298.2 9.7 %all-gather.4 = bf16[4,2,128]{2,1,0:T(2,128)(2,1)S(1)} all-gather(bf16[1,2,128]{2,1,0:T(2,128)(2,1)S(1)} %fusion.49), channel_id=2, replica_groups=mesh['grp'=2,'ep'=4,'tp'=4] {'ep'}, dimensions={0}, use_global_device_ids=true | all-gather | bytes 2560 | tf_op jit(solution)/shard_map/all_gather | solution.py:17
  307.9 13.8 %all-gather.1 = bf16[8,128,128]{2,1,0:T(8,128)(2,1)S(1)} all-gather(bf16[2,128,128]{2,1,0:T(8,128)(2,1)S(1)} %convert_element_type.134), channel_id=3, replica_groups=mesh['grp'=2,'ep'=4,'tp'=4] {'ep'}, dimensions={0}, use_global_device_ids=true | all-gather | bytes 327680 | tf_op jit(solution)/shard_map/all_gather | solution.py:17
  322.4 2.8 multiply_reduce_fusion.1
  325.4 3.3 convolution_convert_fusion.1
  328.7 4.4 %all-to-all-start.1 = ((bf16[4,96,2048]{2,1,0:T(8,128)(2,1)}), bf16[4,96,2048]{2,1,0:T(8,128)(2,1)}, u32[]{:S(2)}, u32[]{:S(2)}) async-start(bf16[4,96,2048]{2,1,0:T(8,128)(2,1)} %bitcast.197), calls=%async_computation.3 | async-start | bytes 3145728 | tf_op jit(solution)/shard_map/all_to_all | solution.py:201
  333.2 27.1 %all-to-all-done.1 = bf16[4,96,2048]{2,1,0:T(8,128)(2,1)} async-done(((bf16[4,96,2048]{2,1,0:T(8,128)(2,1)}), bf16[4,96,2048]{2,1,0:T(8,128)(2,1)}, u32[]{:S(2)}, u32[]{:S(2)}) %all-to-all-start.1) | async-done | bytes 1572896 | tf_op jit(solution)/shard_map/all_to_all | solution.py:201
  360.3 4.1 %gather_fusion.1 = bf16[256,2048]{1,0:T(8,128)(2,1)S(1)} fusion(bf16[384,2048]{1,0:T(8,128)(2,1)} %bitcast.43, s32[1024]{0:T(1024)S(1)} %pad_clamp_fusion), kind=kCustom, calls=%fused_computation.1 | custom fusion | bytes 2098176 | tf_op jit(solution)/shard_map/gather | solution.py:202
  364.5 2.4 reshape.232
  366.8 5.6 %multiply_reduce_fusion = bf16[128,2048]{1,0:T(8,128)(2,1)} fusion(f32[128,2,2048]{2,1,0:T(2,128)} %reshape.232, f32[128,2]{1,0:T(8,128)S(1)} %copy.159), kind=kLoop, calls=%fused_computation.26 | loop fusion | flops 786432 | bytes 2622464 | tf_op jit(solution)/shard_map/reduce_sum | solution.py:203
  (185 shorter events, 61.2 us)
Async XLA Ops:
  7.2 150.8 %copy-start = (bf16[1,512,2048]{2,1,0:T(8,128)(2,1)S(1)}, bf16[1,512,2048]{2,1,0:T(8,128)(2,1)}, u32[]{:S(2)}) copy-start(bf16[1,512,2048]{2,1,0:T(8,128)(2,1)} %param.35) | copy-start | bytes 6291460
  22.9 7.9 %copy-start.17 = (bf16[1024,256]{1,0:T(8,128)(2,1)S(1)}, bf16[1024,256]{1,0:T(8,128)(2,1)}, u32[]{:S(2)}) copy-start(bf16[1024,256]{1,0:T(8,128)(2,1)} %param.23) | copy-start | bytes 1572868
  22.9 8.1 %copy-start.19 = (f32[2,256]{1,0:T(2,128)S(1)}, f32[2,256]{1,0:T(2,128)}, u32[]{:S(2)}) copy-start(f32[2,256]{1,0:T(2,128)} %param.25) | copy-start | bytes 6148
  22.9 121.6 %all-to-all-start = ((bf16[16,96,2048]{2,1,0:T(8,128)(2,1)}), bf16[16,96,2048]{2,1,0:T(8,128)(2,1)}, u32[]{:S(2)}, u32[]{:S(2)}) async-start(bf16[16,96,2048]{2,1,0:T(8,128)(2,1)} %bitcast.178), calls=%async_computation.1 | async-start | bytes 12582912 | tf_op jit(solution)/shard_map/all_to_all | solution.py:178
  30.5 298.2 %reduce-scatter.5.cloned.1.call-start = ((), (), s32[]{:S(2)}) async-start(), calls=%async_computation.5 | async-start | bytes 7864320 | tf_op jit(solution)/shard_map/reduce_scatter | solution.py:195
  33.4 1.6 copy-start.18
  36.8 15.7 %copy-start.7 = (f32[8,128,2,128]{3,0,1,2:T(8,128)}, f32[8,128,2,128]{3,0,1,2:T(8,128)S(1)}, u32[]{:S(2)}) copy-start(f32[8,128,2,128]{3,0,1,2:T(8,128)S(1)} %fusion.31) | copy-start | bytes 3145732
  55.9 2.4 copy-start.6
  144.6 6.3 %copy-start.22 = (bf16[1,2048,512]{2,1,0:T(8,128)(2,1)S(1)}, bf16[1,2048,512]{2,1,0:T(8,128)(2,1)}, u32[]{:S(2)}) copy-start(bf16[1,2048,512]{2,1,0:T(8,128)(2,1)} %param.34) | copy-start | bytes 6291460
  163.3 1.2 copy-start.14
  163.3 1.5 copy-start.15
  163.3 209.4 %reduce-scatter.3.cloned.1.call-start = ((), (), s32[]{:S(2)}) async-start(), calls=%async_computation.4 | async-start | bytes 5242880 | tf_op jit(solution)/shard_map/reduce_scatter | solution.py:183
  167.0 4.0 %copy-start.13 = (f32[1024,256]{0,1:T(8,128)S(1)}, f32[1024,256]{0,1:T(8,128)}, u32[]{:S(2)}) copy-start(f32[1024,256]{0,1:T(8,128)} %get-tuple-element.462) | copy-start | bytes 3145732
  174.1 11.8 %copy-start.2 = (f32[1024,256]{0,1:T(8,128)S(1)}, f32[1024,256]{0,1:T(8,128)}, u32[]{:S(2)}) copy-start(f32[1024,256]{0,1:T(8,128)} %get-tuple-element.461) | copy-start | bytes 3145732
  176.1 1.0 copy-start.8
  187.4 9.2 %copy-start.4 = (f32[1024,2,128]{0,2,1:T(8,128)}, f32[1024,2,128]{0,2,1:T(8,128)S(1)}, u32[]{:S(2)}) copy-start(f32[1024,2,128]{0,2,1:T(8,128)S(1)} %reverse.3) | copy-start | bytes 3145732
  210.2 14.8 %copy-start.11 = (f32[8,128,2,128]{3,1,2,0:T(8,128)S(1)}, f32[8,128,2,128]{3,1,2,0:T(8,128)}, u32[]{:S(2)}) copy-start(f32[8,128,2,128]{3,1,2,0:T(8,128)} %convolution_bitcast_fusion.2) | copy-start | bytes 3145732
  228.4 3.0 copy-start.10
  231.4 49.8 %copy-start.5 = (f32[1024,2,128]{0,2,1:T(8,128)S(1)}, f32[1024,2,128]{0,2,1:T(8,128)}, u32[]{:S(2)}) copy-start(f32[1024,2,128]{0,2,1:T(8,128)} %copy-done.4) | copy-start | bytes 3145732
  281.2 13.0 %copy-start.9 = (f32[8,128,2,128]{3,0,1,2:T(8,128)S(1)}, f32[8,128,2,128]{3,0,1,2:T(8,128)}, u32[]{:S(2)}) copy-start(f32[8,128,2,128]{3,0,1,2:T(8,128)} %get-tuple-element.446) | copy-start | bytes 3145732
  294.3 28.1 %copy-start.3 = (f32[1024,256]{0,1:T(8,128)S(1)}, f32[1024,256]{0,1:T(8,128)}, u32[]{:S(2)}) copy-start(f32[1024,256]{0,1:T(8,128)} %get-tuple-element.461) | copy-start | bytes 3145732
  295.5 26.9 %copy-start.12 = (f32[1024,2,128]{0,2,1:T(8,128)S(1)}, f32[1024,2,128]{0,2,1:T(8,128)}, u32[]{:S(2)}) copy-start(f32[1024,2,128]{0,2,1:T(8,128)} %copy.137) | copy-start | bytes 3145732
  322.4 2.8 copy-start.21
  322.4 3.0 copy-start.16
  328.7 4.4 %copy-start.20 = (f32[128,2]{0,1:T(2,128)S(1)}, f32[128,2]{0,1:T(2,128)}, u32[]{:S(2)}) copy-start(f32[128,2]{0,1:T(2,128)} %param.32) | copy-start | bytes 3076
  328.7 31.6 %all-to-all-start.1 = ((bf16[4,96,2048]{2,1,0:T(8,128)(2,1)}), bf16[4,96,2048]{2,1,0:T(8,128)(2,1)}, u32[]{:S(2)}, u32[]{:S(2)}) async-start(bf16[4,96,2048]{2,1,0:T(8,128)(2,1)} %bitcast.197), calls=%async_computation.3 | async-start | bytes 3145728 | tf_op jit(solution)/shard_map/all_to_all | solution.py:201
  360.3 12.5 %copy-start.1 = (bf16[1,512,2048]{2,1,0:T(8,128)(2,1)S(1)}, bf16[1,512,2048]{2,1,0:T(8,128)(2,1)}, u32[]{:S(2)}) copy-start(bf16[1,512,2048]{2,1,0:T(8,128)(2,1)} %param.35) | copy-start | bytes 6291460
Sparse Core Ops, SparseCore 0:
  163.5 82.2 reduce-scatter.4
  328.8 43.8 reduce-scatter.2
where the time goes:
time: 386 us; the launch traced here: 380 us
  waiting for transfers between devices  94.8 us (25%)
  local copies, waits for them, and re-layouts  84.8 us (22%)
  blocking collectives  68.7 us (18%)
  other arithmetic  55.6 us (14%)
  matrix products  47.5 us (12%)
  between operations  14.8 us (4%)
  starting transfers between devices  12.3 us (3%)
    all_gather x4, blocking collectives, carried_in(): lax.all_gather(part.astype(kind), axis)  68.7 us
    all_to_all x1, waiting for transfers between devices, body(): lax.all_to_all(copies, ('ep', 'tp'), split_axis=0, concat_axis=0, tiled=T...  67.3 us
    all_to_all x1, waiting for transfers between devices, body(): lax.all_to_all(expert_sum, 'ep', split_axis=0, concat_axis=0, tiled=True)  27.1 us
    add x16, other arithmetic, advance(): return (state * decay[..., None] + increment, state)  16.3 us
    unnamed x55, local copies, waits for them, and re-layouts  11.4 us
    dynamic_update_slice x16, other arithmetic, local_recurrence(): lax.scan(advance, initial, (jnp.exp(block_last), increments))  10.6 us
    rev x1, local copies, waits for them, and re-layouts, mixer_head_states(): jnp.flip(output + jnp.einsum('lhd,hdv->lhv', carried, entering, precision...  9.37 us
    rev x2, local copies, waits for them, and re-layouts, mixer_head_states(): jnp.flip(ending_state, 0)  8.89 us
  transfers between devices with their start and end apart: 4, of which 3 were waited for; matrix products, arithmetic and copies ran while one was open for 40% of the time, Pallas kernels for 0%

commit v1 on v0

--- a/solution.py
+++ b/solution.py
@@ -9,6 +9,20 @@
 CLAMP_LIMIT = 7.0
 SIGMOID_SCALE = 1.702
 PRECISE = lax.Precision.HIGHEST
+
+
+def test_wires(block_here, which_dim, target):
+    clean = block_here.shape
+    u_next = block_here.reshape(
+        *clean[:which_dim], target, clean[which_dim] // target, *clean[which_dim + 1 :]
+    )
+    return jnp.moveaxis(u_next, which_dim, 0)
+
+
+def switch_scales(t0, dim_no):
+    opened = list(t0.shape[1:])
+    opened[dim_no] *= t0.shape[0]
+    return jnp.moveaxis(t0, 0, dim_no).reshape(opened)
 
 
 def carried_in(value, axis, combine, identity, reverse):
@@ -198,7 +212,17 @@
         scatter_dimension=0,
         tiled=True,
     )
-    returned = lax.all_to_all(expert_sum, "ep", split_axis=0, concat_axis=0, tiled=True)
+    front, val2 = (lax.psum(1, axis_name="ep"), lax.axis_index("ep"))
+    found_now = test_wires(expert_sum, 0, front)
+    res = found_now
+    for u in range(1, front):
+        near, out_arr = ((val2 + u) % front, (val2 - u) % front)
+        next_value = lax.dynamic_index_in_dim(found_now, near, 0)
+        item_now = lax.ppermute(
+            next_value, axis_name="ep", perm=tuple(((dd, (dd + u) % front) for dd in range(front)))
+        )
+        res = lax.dynamic_update_slice_in_dim(res, item_now, out_arr, axis=0)
+    returned = switch_scales(res, 0)
     gathered = returned[destination].reshape(tokens, top_count, features)
     moe_out = jnp.sum(
         chosen_expert_weight[:, :, None] * gathered.astype(jnp.float32), axis=1

time: 386 us -> 366 us (0.948)
  waiting for transfers between devices: 94.8 us -> 68.8 us
    all_to_all x1 -> x0, waiting for transfers between devices: 27.1 us -> none  [body(): lax.all_to_all(expert_sum, 'ep', split_axis=0, concat_axis=0, tiled=True)]
    ppermute x0 -> x3, waiting for transfers between devices: none -> 24 us  [body(): lax.ppermute(next_value, axis_name='ep', perm=tuple(((dd, (dd + u) % fron...]
    all_to_all x1, waiting for transfers between devices: 67.3 us -> 44.8 us  [body(): lax.all_to_all(copies, ('ep', 'tp'), split_axis=0, concat_axis=0, tiled=T...]
    ppermute x0 -> x3, starting transfers between devices: none -> 6.35 us  [body(): lax.ppermute(next_value, axis_name='ep', perm=tuple(((dd, (dd + u) % fron...]
    rev x2, local copies, waits for them, and re-layouts: 2.99 us -> 7.85 us  [mixer_head_states(): jnp.flip(forget_log_rates, 0)]
    another operation x5, local copies, waits for them, and re-layouts: 3.75 us -> 8.47 us
    exp x4, local copies, waits for them, and re-layouts: 7.57 us -> 3.05 us  [local_recurrence(): jnp.exp(cumul + offsets[:, None])]
    all_to_all x1 -> x0, starting transfers between devices: 4.35 us -> none  [body(): lax.all_to_all(expert_sum, 'ep', split_axis=0, concat_axis=0, tiled=True)]
  transfers between devices with their start and end apart: 4 -> 6, of which waited for: 3 -> 4; matrix products, arithmetic and copies ran while one was open for 40% -> 42% of each run, Pallas kernels for 0% -> 0%
where the time goes in v1:
time: 366 us; the launch traced here: 359 us
  local copies, waits for them, and re-layouts  88.4 us (24%)
  blocking collectives  69.1 us (19%)
  waiting for transfers between devices  68.8 us (19%)
  other arithmetic  55.3 us (15%)
  matrix products  47.7 us (13%)
  between operations  14.9 us (4%)
  starting transfers between devices  14 us (4%)
    all_gather x4, blocking collectives, carried_in(): lax.all_gather(part.astype(kind), axis)  69.1 us
    all_to_all x1, waiting for transfers between devices, body(): lax.all_to_all(copies, ('ep', 'tp'), split_axis=0, concat_axis=0, tiled=T...  44.8 us
    ppermute x3, waiting for transfers between devices, body(): lax.ppermute(next_value, axis_name='ep', perm=tuple(((dd, (dd + u) % fron...  24 us
    add x16, other arithmetic, advance(): return (state * decay[..., None] + increment, state)  16.3 us
    unnamed x53, local copies, waits for them, and re-layouts  11.1 us
    dynamic_update_slice x16, other arithmetic, local_recurrence(): lax.scan(advance, initial, (jnp.exp(block_last), increments))  10.7 us
    rev x2, local copies, waits for them, and re-layouts, mixer_head_states(): jnp.flip(ending_state, 0)  8.82 us
    another operation x5, local copies, waits for them, and re-layouts  8.47 us
  transfers between devices with their start and end apart: 6, of which 4 were waited for; matrix products, arithmetic and copies ran while one was open for 42% of the time, Pallas kernels for 0%

profile of v1, /device:TPU:0, one launch (start us, length us, event | category | flops | bytes accessed | tf_op | source)
XLA Modules:
  0.0 359.4 jit_solution(4689369173254179662)
XLA Ops:
  11.0 1.4 scatter_custom_fusion
  15.0 3.1 gather_fusion
  18.0 4.9 %broadcast_in_dim.32 = bf16[4,4,96,2048]{3,2,1,0:T(8,128)(2,1)} broadcast(bf16[4,96,2048]{2,1,0:T(8,128)(2,1)} %bitcast.186), dimensions={0,2,3} | broadcast | bytes 7864320 | tf_op jit(solution)/shard_map/broadcast_in_dim | solution.py:189
  22.9 7.6 %all-to-all-start = ((bf16[16,96,2048]{2,1,0:T(8,128)(2,1)}), bf16[16,96,2048]{2,1,0:T(8,128)(2,1)}, u32[]{:S(2)}, u32[]{:S(2)}) async-start(bf16[16,96,2048]{2,1,0:T(8,128)(2,1)} %bitcast.181), calls=%async_computation.1 | async-start | bytes 12582912 | tf_op jit(solution)/shard_map/all_to_all | solution.py:192
  30.8 2.4 log-plus-one_bitcast_fusion
  33.3 6.3 %rev.17 = f32[1024,2,128]{0,2,1:T(8,128)} reverse(f32[1024,2,128]{0,2,1:T(8,128)S(1)} %broadcast_add_fusion), dimensions={0} | reverse | bytes 2097152 | tf_op jit(solution)/shard_map/jit(_flip)/rev | solution.py:133
  39.6 1.5 copy.139
  42.8 7.5 %rev.18 = f32[1024,2,128]{0,2,1:T(8,128)S(1)} reverse(f32[1024,2,128]{0,2,1:T(8,128)} %bitcast.196), dimensions={0} | reverse | bytes 2097152 | tf_op jit(solution)/shard_map/jit(_flip)/rev | solution.py:131
  51.6 2.0 copy.118
  53.7 2.4 multiply_bitcast_fusion
  56.1 6.1 %reverse.3 = f32[1024,2,128]{0,2,1:T(8,128)} reverse(f32[1024,2,128]{0,2,1:T(8,128)S(1)} %bitcast.184), dimensions={0} | reverse | bytes 2097152 | tf_op jit(solution)/shard_map/reverse
  62.2 2.3 broadcast_multiply_fusion.1
  64.5 2.6 copy.138
  68.4 5.9 %rev.19 = f32[1024,2,128]{0,2,1:T(8,128)} reverse(bf16[1024,2,128]{0,2,1:T(8,128)(2,1)S(1)} %bitcast.199), dimensions={0} | reverse | bytes 1572864 | tf_op jit(solution)/shard_map/jit(_flip)/rev | solution.py:132
  74.3 1.5 copy.147
  77.3 4.7 %exponential_multiply_fusion = (f32[8,128,2,128]{3,0,1,2:T(8,128)S(1)}, f32[8,128,2,128]{3,0,1,2:T(8,128)}, f32[8,128,2,128]{3,0,1,2:T(8,128)}, f32[8,128,2,128]{3,0,1,2:T(8,128)}) fusion(f32[8,128,2,128]{3,0,1,2:T(8,128)} %copy-done.6, f32[8,128,2,128]{3,1,0,2:T(8,128)} %bitcast.187, f32[8,2,128]{2,0,1:T(8,128)S(1)} %get-tuple-element.456, ...), kind=kLoop, calls=%fused_computation.63 | loop fusion | flops 1572864 | bytes 7356416 | tf_op jit(solution)/shard_map/mul | solution.py:72
  82.0 2.9 fusion.20
  86.0 13.7 %while.58 = (s32[]{:T(128)}, f32[2,128,128]{2,1,0:T(8,128)S(1)}, f32[8,2,128,128]{3,2,1,0:T(8,128)}, f32[8,2,128]{2,0,1:T(8,128)S(1)}, f32[8,2,128,128]{3,2,1,0:T(8,128)}, /*index=5*/s32[]{:T(128)}, s32[]{:T(128)}) while((s32[]{:T(128)}, f32[2,128,128]{2,1,0:T(8,128)S(1)}, f32[8,2,128,128]{3,2,1,0:T(8,128)}, ...), condition=%wide.region_9.10_spmd.clone, body=%wide.region_8.9_spmd.clone.sunk | while | flops 131075 | bytes 659040 | solution.py:83
  99.7 44.8 %all-to-all-done = bf16[16,96,2048]{2,1,0:T(8,128)(2,1)} async-done(((bf16[16,96,2048]{2,1,0:T(8,128)(2,1)}), bf16[16,96,2048]{2,1,0:T(8,128)(2,1)}, u32[]{:S(2)}, u32[]{:S(2)}) %all-to-all-start) | async-done | bytes 6291488 | tf_op jit(solution)/shard_map/all_to_all | solution.py:192
  144.6 6.3 %convolution_minimum_fusion = f32[1536,512]{1,0:T(8,128)S(1)} fusion(bf16[1536,2048]{1,0:T(8,128)(2,1)} %bitcast.35, bf16[1,2048,512]{2,1,0:T(8,128)(2,1)} %param.33), kind=kOutput, calls=%fused_computation.18 | convolution fusion | flops 3222011904 | bytes 11534336 | tf_op jit(solution)/shard_map/dot_general | solution.py:193
  150.9 6.9 %fusion.5 = bf16[1536,512]{1,0:T(8,128)(2,1)S(1)} fusion(f32[1536,512]{1,0:T(8,128)S(1)} %convolution_minimum_fusion, bf16[1536,2048]{1,0:T(8,128)(2,1)} %bitcast.35, bf16[1,2048,512]{2,1,0:T(8,128)(2,1)S(1)} %copy-done.21), kind=kOutput, calls=%fused_computation.22 | convolution fusion | flops 3228303360 | bytes 13107200 | tf_op jit(solution)/shard_map/dot_general | solution.py:194
  157.9 5.9 %convolution_convert_fusion = bf16[1536,2048]{1,0:T(8,128)(2,1)} fusion(bf16[1536,512]{1,0:T(8,128)(2,1)S(1)} %bitcast.201, bf16[1,512,2048]{2,1,0:T(8,128)(2,1)S(1)} %copy-done), kind=kOutput, calls=%fused_computation.15 | convolution fusion | flops 3224371200 | bytes 9961472 | tf_op jit(solution)/shard_map/dot_general | solution.py:210
  165.1 4.6 %convolution_multiply_fusion = f32[8,2,128,128]{3,2,1,0:T(8,128)} fusion(f32[8,128,2,128]{3,0,1,2:T(8,128)} %get-tuple-element.445, f32[8,128,2,128]{3,0,1,2:T(8,128)S(1)} %copy-done.2, f32[128,128]{1,0:T(8,128)S(1)} %fusion.43), kind=kOutput, calls=%fused_computation.32 | convolution fusion | flops 402915328 | bytes 3211264 | tf_op jit(solution)/shard_map/nchd,nshd->nhcs/dot_general | solution.py:74
  170.9 2.5 convolution_bitcast_fusion.2
  173.4 2.2 fusion.10
  175.6 1.7 copy.154
  180.0 31.6 %all-gather.5 = bf16[4,2,128]{2,1,0:T(2,128)(2,1)S(1)} all-gather(bf16[1,2,128]{2,1,0:T(2,128)(2,1)S(1)} %fusion.50), channel_id=4, replica_groups=mesh['grp'=2,'ep'=4,'tp'=4] {'ep'}, dimensions={0}, use_global_device_ids=true | all-gather | bytes 2560 | tf_op jit(solution)/shard_map/all_gather | solution.py:31
  211.6 14.0 %all-gather.3 = bf16[8,128,128]{2,1,0:T(8,128)(2,1)S(1)} all-gather(bf16[2,128,128]{2,1,0:T(8,128)(2,1)S(1)} %convert_element_type.137), channel_id=5, replica_groups=mesh['grp'=2,'ep'=4,'tp'=4] {'ep'}, dimensions={0}, use_global_device_ids=true | all-gather | bytes 327680 | tf_op jit(solution)/shard_map/all_gather | solution.py:31
  226.6 2.6 fusion.9
  229.2 6.0 %rev.20 = f32[1024,2,128]{0,2,1:T(8,128)} reverse(f32[1024,2,128]{0,2,1:T(8,128)S(1)} %fusion.9), dimensions={0} | reverse | bytes 2097152 | tf_op jit(solution)/shard_map/jit(_flip)/rev | solution.py:136
  238.3 2.5 copy.123
  242.0 2.6 copy.122
  244.7 3.1 exponential_multiply_fusion.2
  247.8 2.4 convolution_multiply_fusion.1
  250.9 2.0 fusion.25
  254.1 13.7 %while.56 = (s32[]{:T(128)}, f32[2,128,128]{2,1,0:T(8,128)S(1)}, f32[8,2,128,128]{3,2,1,0:T(8,128)}, f32[8,2,128]{2,0,1:T(8,128)S(1)}, f32[8,2,128,128]{3,2,1,0:T(8,128)}, /*index=5*/s32[]{:T(128)}, s32[]{:T(128)}) while((s32[]{:T(128)}, f32[2,128,128]{2,1,0:T(8,128)S(1)}, f32[8,2,128,128]{3,2,1,0:T(8,128)}, ...), condition=%wide.region_2.3_spmd.clone, body=%wide.region_1.2_spmd.clone.sunk | while | flops 131075 | bytes 659040 | solution.py:83
  267.8 2.4 fusion.13
  273.3 9.7 %all-gather.4 = bf16[4,2,128]{2,1,0:T(2,128)(2,1)S(1)} all-gather(bf16[1,2,128]{2,1,0:T(2,128)(2,1)S(1)} %fusion.49), channel_id=2, replica_groups=mesh['grp'=2,'ep'=4,'tp'=4] {'ep'}, dimensions={0}, use_global_device_ids=true | all-gather | bytes 2560 | tf_op jit(solution)/shard_map/all_gather | solution.py:31
  283.0 13.8 %all-gather.1 = bf16[8,128,128]{2,1,0:T(8,128)(2,1)S(1)} all-gather(bf16[2,128,128]{2,1,0:T(8,128)(2,1)S(1)} %convert_element_type.134), channel_id=3, replica_groups=mesh['grp'=2,'ep'=4,'tp'=4] {'ep'}, dimensions={0}, use_global_device_ids=true | all-gather | bytes 327680 | tf_op jit(solution)/shard_map/all_gather | solution.py:31
  297.7 3.0 multiply_reduce_fusion.1
  301.9 3.3 convolution_convert_fusion.1
  306.4 13.8 %collective-permute-done = bf16[1,96,2048]{2,1,0:T(8,128)(2,1)S(1)} collective-permute-done((bf16[1,96,2048]{2,1,0:T(8,128)(2,1)S(1)}, bf16[1,96,2048]{2,1,0:T(8,128)(2,1)S(1)}, u32[]{:S(2)}, u32[]{:S(2)}) %collective-permute-start) | collective-permute-done | bytes 393248 | tf_op jit(solution)/shard_map/ppermute | solution.py:221
  320.2 2.0 constant_dynamic-slice_fusion.2
  322.2 5.9 %collective-permute-start.1 = (bf16[1,96,2048]{2,1,0:T(8,128)(2,1)S(1)}, bf16[1,96,2048]{2,1,0:T(8,128)(2,1)S(1)}, u32[]{:S(2)}, u32[]{:S(2)}) collective-permute-start(bf16[1,96,2048]{2,1,0:T(8,128)(2,1)S(1)} %get-tuple-element.447), channel_id=1, source_target_pairs={{0,8},{4,12},{8,0},{12,4},{1,9},{5,13},{9,1},{13,5},{2,10},{6,14},... | collective-permute-start | bytes 1179656 | tf_op jit(solution)/shard_map/ppermute | solution.py:221
  328.7 9.5 %collective-permute-done.1 = bf16[1,96,2048]{2,1,0:T(8,128)(2,1)S(1)} collective-permute-done((bf16[1,96,2048]{2,1,0:T(8,128)(2,1)S(1)}, bf16[1,96,2048]{2,1,0:T(8,128)(2,1)S(1)}, u32[]{:S(2)}, u32[]{:S(2)}) %collective-permute-start.1) | collective-permute-done | bytes 393248 | tf_op jit(solution)/shard_map/ppermute | solution.py:221
  340.4 4.0 %gather_fusion.1 = bf16[256,2048]{1,0:T(8,128)(2,1)S(1)} fusion(bf16[384,2048]{1,0:T(8,128)(2,1)} %bitcast.180, s32[1024]{0:T(1024)S(1)} %pad_clamp_fusion), kind=kCustom, calls=%fused_computation.1 | custom fusion | bytes 2098176 | tf_op jit(solution)/shard_map/gather | solution.py:226
  344.4 2.3 reshape.238
  346.7 5.6 %multiply_reduce_fusion = bf16[128,2048]{1,0:T(8,128)(2,1)} fusion(f32[128,2,2048]{2,1,0:T(2,128)} %reshape.238, f32[128,2]{1,0:T(8,128)S(1)} %copy.159), kind=kLoop, calls=%fused_computation.26 | loop fusion | flops 786432 | bytes 2622464 | tf_op jit(solution)/shard_map/reduce_sum | solution.py:227
  (192 shorter events, 62.9 us)
Async XLA Ops:
  7.2 150.8 %copy-start = (bf16[1,512,2048]{2,1,0:T(8,128)(2,1)S(1)}, bf16[1,512,2048]{2,1,0:T(8,128)(2,1)}, u32[]{:S(2)}) copy-start(bf16[1,512,2048]{2,1,0:T(8,128)(2,1)} %param.35) | copy-start | bytes 6291460
  22.9 7.6 %copy-start.16 = (bf16[1024,256]{1,0:T(8,128)(2,1)S(1)}, bf16[1024,256]{1,0:T(8,128)(2,1)}, u32[]{:S(2)}) copy-start(bf16[1024,256]{1,0:T(8,128)(2,1)} %param.23) | copy-start | bytes 1572868
  22.9 7.9 %copy-start.18 = (f32[2,256]{1,0:T(2,128)S(1)}, f32[2,256]{1,0:T(2,128)}, u32[]{:S(2)}) copy-start(f32[2,256]{1,0:T(2,128)} %param.25) | copy-start | bytes 6148
  22.9 121.6 %all-to-all-start = ((bf16[16,96,2048]{2,1,0:T(8,128)(2,1)}), bf16[16,96,2048]{2,1,0:T(8,128)(2,1)}, u32[]{:S(2)}, u32[]{:S(2)}) async-start(bf16[16,96,2048]{2,1,0:T(8,128)(2,1)} %bitcast.181), calls=%async_computation.1 | async-start | bytes 12582912 | tf_op jit(solution)/shard_map/all_to_all | solution.py:192
  30.5 274.8 %reduce-scatter.5.cloned.1.call-start = ((), (), s32[]{:S(2)}) async-start(), calls=%async_computation.4 | async-start | bytes 7864320 | tf_op jit(solution)/shard_map/reduce_scatter | solution.py:209
  30.8 2.4 copy-start.17
  41.8 1.0 copy-start.6
  56.1 8.5 %copy-start.3 = (f32[1024,256]{0,1:T(8,128)}, f32[1024,256]{0,1:T(8,128)S(1)}, u32[]{:S(2)}) copy-start(f32[1024,256]{0,1:T(8,128)S(1)} %get-tuple-element.464) | copy-start | bytes 3145732
  144.6 6.3 %copy-start.21 = (bf16[1,2048,512]{2,1,0:T(8,128)(2,1)S(1)}, bf16[1,2048,512]{2,1,0:T(8,128)(2,1)}, u32[]{:S(2)}) copy-start(bf16[1,2048,512]{2,1,0:T(8,128)(2,1)} %param.34) | copy-start | bytes 6291460
  163.8 1.2 copy-start.2
  163.9 188.4 %reduce-scatter.3.cloned.1.call-start = ((), (), s32[]{:S(2)}) async-start(), calls=%async_computation.3 | async-start | bytes 5242880 | tf_op jit(solution)/shard_map/reduce_scatter | solution.py:197
  170.9 2.5 copy-start.14
  175.6 2.9 copy-start.9
  178.7 47.9 %copy-start.5 = (f32[1024,2,128]{0,2,1:T(8,128)S(1)}, f32[1024,2,128]{0,2,1:T(8,128)}, u32[]{:S(2)}) copy-start(f32[1024,2,128]{0,2,1:T(8,128)} %reverse.3) | copy-start | bytes 3145732
  229.1 6.0 %copy-start.13 = (f32[32,8,8,128]{3,1,2,0:T(8,128)S(1)}, f32[32,8,8,128]{3,1,2,0:T(8,128)}, u32[]{:S(2)}) copy-start(f32[32,8,8,128]{3,1,2,0:T(8,128)} %get-tuple-element.459) | copy-start | bytes 3145732
  235.9 1.2 copy-start.12
  236.4 4.5 %copy-start.7 = (f32[8,128,2,128]{3,0,1,2:T(8,128)}, f32[8,128,2,128]{3,0,1,2:T(8,128)S(1)}, u32[]{:S(2)}) copy-start(f32[8,128,2,128]{3,0,1,2:T(8,128)S(1)} %fusion.31) | copy-start | bytes 3145732
  237.2 3.7 %copy-start.11 = (f32[32,8,8,128]{3,1,2,0:T(8,128)S(1)}, f32[32,8,8,128]{3,1,2,0:T(8,128)}, u32[]{:S(2)}) copy-start(f32[32,8,8,128]{3,1,2,0:T(8,128)} %get-tuple-element.463) | copy-start | bytes 3145732
  240.9 3.8 %slice-start = ((f32[8,128,2,128]{3,0,1,2:T(8,128)}), f32[8,1,2,128]{3,0,1,2:T(8,128)S(1)}, s32[]{:S(2)}) async-start(f32[8,128,2,128]{3,0,1,2:T(8,128)} %copy-done.7), calls=%async_computation.5 | async-start | bytes 16384 | tf_op jit(solution)/shard_map/slice | solution.py:69
  240.9 3.8 %copy-start.8 = (f32[8,128,2,128]{3,0,1,2:T(8,128)S(1)}, f32[8,128,2,128]{3,0,1,2:T(8,128)}, u32[]{:S(2)}) copy-start(f32[8,128,2,128]{3,0,1,2:T(8,128)} %copy-done.7) | copy-start | bytes 3145732
  270.3 1.4 copy-start.10
  271.9 25.7 %copy-start.4 = (f32[1024,256]{0,1:T(8,128)S(1)}, f32[1024,256]{0,1:T(8,128)}, u32[]{:S(2)}) copy-start(f32[1024,256]{0,1:T(8,128)} %copy-done.3) | copy-start | bytes 3145732
  297.7 3.1 copy-start.20
  300.7 1.2 copy-start.15
  305.2 23.3 %copy-start.19 = (f32[128,2]{0,1:T(2,128)S(1)}, f32[128,2]{0,1:T(2,128)}, u32[]{:S(2)}) copy-start(f32[128,2]{0,1:T(2,128)} %param.32) | copy-start | bytes 3076
  306.3 13.9 %collective-permute-start = (bf16[1,96,2048]{2,1,0:T(8,128)(2,1)S(1)}, bf16[1,96,2048]{2,1,0:T(8,128)(2,1)S(1)}, u32[]{:S(2)}, u32[]{:S(2)}) collective-permute-start(bf16[1,96,2048]{2,1,0:T(8,128)(2,1)S(1)} %constant_dynamic-slice_fusion.4), channel_id=1, source_target_pairs={{0,4},{4,8},{8,12},{12,0},{1,5},{5,9},{9,13},{13,1},{2,6},{6,10},{... | collective-permute-start | bytes 1179656 | tf_op jit(solution)/shard_map/ppermute | solution.py:221
  322.2 15.9 %collective-permute-start.1 = (bf16[1,96,2048]{2,1,0:T(8,128)(2,1)S(1)}, bf16[1,96,2048]{2,1,0:T(8,128)(2,1)S(1)}, u32[]{:S(2)}, u32[]{:S(2)}) collective-permute-start(bf16[1,96,2048]{2,1,0:T(8,128)(2,1)S(1)} %get-tuple-element.447), channel_id=1, source_target_pairs={{0,8},{4,12},{8,0},{12,4},{1,9},{5,13},{9,1},{13,5},{2,10},{6,14},... | collective-permute-start | bytes 1179656 | tf_op jit(solution)/shard_map/ppermute | solution.py:221
  328.1 11.5 %collective-permute-start.2 = (bf16[1,96,2048]{2,1,0:T(8,128)(2,1)S(1)}, bf16[1,96,2048]{2,1,0:T(8,128)(2,1)S(1)}, u32[]{:S(2)}, u32[]{:S(2)}) collective-permute-start(bf16[1,96,2048]{2,1,0:T(8,128)(2,1)S(1)} %get-tuple-element.446), channel_id=1, source_target_pairs={{0,12},{4,0},{8,4},{12,8},{1,13},{5,1},{9,5},{13,9},{2,14},{6,2},{... | collective-permute-start | bytes 1179656 | tf_op jit(solution)/shard_map/ppermute | solution.py:221
  344.4 7.9 %copy-start.1 = (bf16[1,512,2048]{2,1,0:T(8,128)(2,1)S(1)}, bf16[1,512,2048]{2,1,0:T(8,128)(2,1)}, u32[]{:S(2)}) copy-start(bf16[1,512,2048]{2,1,0:T(8,128)(2,1)} %param.35) | copy-start | bytes 6291460
Sparse Core Ops, SparseCore 0:
  164.0 82.2 reduce-scatter.4
  305.4 43.8 reduce-scatter.2
